TPU v7x, 32 devices: a whole 2x2x4 slice. The times are simulated.
32 devices in a mesh: sp: 16 (over z, y, x), tp: 2 (over core).
Axes of the slice: x: 2, y: 2, z: 4, core: 2. Of those that a mesh axis runs over, the one named last changes fastest.
Arguments:
- tokens: bfloat16 [4096, 2048], P(('sp', 'tp')), may hold values from -6 to 6
- norm_gain: float32 [2048], replicated, may hold values from 0.1 to 1.9
- w_query: bfloat16 [2048, 1024], P('sp', 'tp'), may hold values from -0.125 to 0.125
- w_forget: bfloat16 [2048, 1024], P('sp', 'tp'), may hold values from -0.125 to 0.125
- w_value: bfloat16 [2048, 1024], P('sp', 'tp'), may hold values from -0.125 to 0.125
- w_outgate: bfloat16 [2048, 1024], P('sp', 'tp'), may hold values from -0.125 to 0.125
- leak: float32 [1024], P('tp'), may hold values from 4.8828126e-05 to 0.00024414062
- decay_shift: float32 [4096, 1024], P('sp', 'tp'), may hold values from -1 to 0
- head_gain: float32 [128], replicated, may hold values from 0.1 to 1.9
- w_glu_value: bfloat16 [2048, 2048], P('sp', 'tp'), may hold values from -0.125 to 0.125
- w_glu_gate: bfloat16 [2048, 2048], P('sp', 'tp'), may hold values from -0.125 to 0.125
- conv_kernel: float32 [31, 2048], P(None, 'tp'), may hold values from -20 to 20
- ln_gain: float32 [2048], P('tp'), may hold values from 0.1 to 1.9
- ln_bias: float32 [2048], P('tp'), may hold values from -3 to 3
- w_out_rec: bfloat16 [1024, 2048], P('tp', 'sp'), may hold values from -0.125 to 0.125
- w_out_conv: bfloat16 [2048, 2048], P('tp', 'sp'), may hold values from -0.09375 to 0.09375
Outputs:
- mixed: bfloat16 [4096, 2048], P(('sp', 'tp'))
All inputs are finite; a program needn't handle non-finite values.
Results may differ from a plain program's by a relative error of at most 0.019.
Values may be sent and summed in bfloat16 or wider, within the bound.
A program may use at most 64 MiB of HBM per device.

v0:
```python
import jax
import jax.numpy as jnp
from jax import lax
from jax.sharding import PartitionSpec as P

HEAD_K = 128
HEAD_V = 128
KERNEL = 31
BLOCK = 64
exact_precision = lax.Precision.HIGHEST


def prefix(value, axis, combine, identity):
    peers, position = (lax.axis_size(axis), lax.axis_index(axis))
    everything = jax.tree.map(
        lambda part, kind: lax.all_gather(part.astype(kind), axis),
        value,
        (jnp.bfloat16, jnp.bfloat16),
    )
    start = jax.tree.map(
        lambda part, zero: jnp.broadcast_to(jnp.asarray(zero, part.dtype), part.shape),
        value,
        identity,
    )

    def turn(k, before):
        reached = k < position
        new = combine(
            before, jax.tree.map(lambda part, own: part[k].astype(own.dtype), everything, value)
        )
        return jax.tree.map(lambda a, b: jnp.where(reached, a, b), new, before)

    return lax.fori_loop(0, peers, turn, start)


def from_behind(value, axis, steps):
    count = lax.axis_size(axis)
    initial, last = (max(0, -steps), min(count, count - steps))
    return lax.ppermute(value, axis, [(source, source + steps) for source in range(initial, last)])


def normalize(row_block, norm_gain):
    values_in = row_block.astype(jnp.float32)
    row_scale = lax.rsqrt(jnp.mean(values_in * values_in, axis=1, keepdims=True) + 1e-06)
    return (values_in * row_scale * norm_gain).astype(jnp.bfloat16)


def combine_states(earlier, later):
    return (earlier[0] + later[0], jnp.exp(later[0])[..., None] * earlier[1] + later[1])


def local_recurrence(queries, in_gate, payload_matrix_lines, log_decay):
    row_count, head_count, key_width = queries.shape
    value_width = payload_matrix_lines.shape[2]
    block_count = row_count // BLOCK

    def split_blocks(tensor):
        return tensor.reshape(block_count, BLOCK, head_count, tensor.shape[-1])

    q_blocks = split_blocks(queries)
    k_blocks = split_blocks(in_gate)
    v_blocks = split_blocks(payload_matrix_lines)
    cumulative_sum = jnp.cumsum(split_blocks(log_decay), axis=1)
    causal = jnp.tril(jnp.ones((BLOCK, BLOCK), jnp.float32))
    scores = jnp.einsum(
        "nthk,nshk->nhts",
        q_blocks * jnp.exp(cumulative_sum),
        k_blocks * jnp.exp(-cumulative_sum),
        precision=exact_precision,
    )
    within = jnp.einsum("nhts,nshv->nthv", scores * causal, v_blocks, precision=exact_precision)
    block_finish = cumulative_sum[:, -1]
    contrib = jnp.einsum(
        "nshk,nshv->nhkv",
        k_blocks * jnp.exp(block_finish[:, None] - cumulative_sum),
        v_blocks,
        precision=exact_precision,
    )

    def advance(carried_in, inputs):
        state_list, before = carried_in
        query_block, column_block, e_block, added_terms = inputs
        carried_state = jnp.einsum(
            "aub,ubd->aud",
            query_block * jnp.exp(column_block),
            state_list,
            precision=exact_precision,
        )
        device_query = query_block * jnp.exp(column_block + before[None])
        state_list = jnp.exp(e_block)[..., None] * state_list + added_terms
        return ((state_list, before + e_block), (carried_state, device_query))

    initial = (
        jnp.zeros((head_count, key_width, value_width), jnp.float32),
        jnp.zeros((head_count, key_width), jnp.float32),
    )
    (state_list, totals), (carried_state, device_query) = lax.scan(
        advance, initial, (q_blocks, cumulative_sum, block_finish, contrib)
    )
    recurrence_step = (within + carried_state).reshape(row_count, head_count, value_width)
    return (
        recurrence_step,
        device_query.reshape(row_count, head_count, key_width),
        state_list,
        totals,
    )


def on_device(
    tokens,
    norm_gain,
    w_query,
    w_forget,
    w_value,
    w_outgate,
    leak,
    decay_shift,
    head_gain,
    w_glu_value,
    w_glu_gate,
    conv_kernel,
    ln_gain,
    ln_bias,
    w_out_rec,
    w_out_conv,
):
    widths = [
        w_query.shape[1],
        w_forget.shape[1],
        w_value.shape[1],
        w_outgate.shape[1],
        w_glu_value.shape[1],
        w_glu_gate.shape[1],
    ]
    gathered = (
        lax.all_gather(w_query, "sp", axis=0, tiled=True),
        lax.all_gather(w_forget, "sp", axis=0, tiled=True),
        lax.all_gather(w_value, "sp", axis=0, tiled=True),
        lax.all_gather(w_outgate, "sp", axis=0, tiled=True),
        lax.all_gather(w_glu_value, "sp", axis=0, tiled=True),
        lax.all_gather(w_glu_gate, "sp", axis=0, tiled=True),
        lax.all_gather(w_out_rec, "sp", axis=1, tiled=True),
        lax.all_gather(w_out_conv, "sp", axis=1, tiled=True),
    )
    full_in = gathered[:6]
    out_rec = gathered[6]
    out_conv = gathered[7]
    normed = normalize(lax.all_gather(tokens, "tp", axis=0, tiled=True), norm_gain)
    joined = jnp.concatenate(
        [
            jnp.dot(normed, weight, preferred_element_type=jnp.float32).astype(jnp.bfloat16)
            for weight in full_in
        ],
        axis=1,
    )
    projections = []
    column = 0
    for width_now in widths:
        projections.append(joined[:, column : column + width_now])
        column = column + width_now
    query_pre, forget_pre, value_pre, gate_pre, glu_value_pre, glu_gate_pre = projections
    row_count = query_pre.shape[0]
    head_count = query_pre.shape[1] // HEAD_K
    queries = jax.nn.silu(query_pre.astype(jnp.float32))
    in_gate = leak * jax.nn.sigmoid(-forget_pre.astype(jnp.float32))
    log_decay = jnp.log1p(-in_gate) + decay_shift
    recurrence_step, device_query, state_list, totals = local_recurrence(
        queries.reshape(row_count, head_count, HEAD_K),
        in_gate.reshape(row_count, head_count, HEAD_K),
        value_pre.astype(jnp.float32).reshape(row_count, head_count, HEAD_V),
        log_decay.reshape(row_count, head_count, HEAD_K),
    )
    _, incoming_state = prefix(
        (totals, state_list),
        "sp",
        combine_states,
        (jnp.zeros_like(totals), jnp.zeros_like(state_list)),
    )
    recurrence_step = recurrence_step + jnp.einsum(
        "aub,ubd->aud", device_query, incoming_state, precision=exact_precision
    )
    scaling = lax.rsqrt(jnp.mean(recurrence_step * recurrence_step, axis=2, keepdims=True) + 1e-06)
    gate_act = jax.nn.silu(gate_pre.astype(jnp.float32)).reshape(row_count, head_count, HEAD_V)
    head_out = (
        (recurrence_step * scaling * head_gain * gate_act)
        .reshape(row_count, head_count * HEAD_V)
        .astype(jnp.bfloat16)
    )
    glu = (
        glu_value_pre.astype(jnp.float32) * jax.nn.sigmoid(glu_gate_pre.astype(jnp.float32))
    ).astype(jnp.bfloat16)
    left_rim = from_behind(glu[row_count - (KERNEL - 1) :], "sp", 1)
    extended = jnp.concatenate([left_rim, glu], axis=0).astype(jnp.float32)

    def add_tap(tap_index, accum):
        taps = lax.dynamic_slice_in_dim(conv_kernel, tap_index, 1, 0)
        return accum + taps * lax.dynamic_slice_in_dim(extended, tap_index, row_count, 0)

    conv_sum = lax.fori_loop(0, KERNEL, add_tap, jnp.zeros((row_count, glu.shape[1]), jnp.float32))
    channel_count = conv_sum.shape[1] * lax.axis_size("tp")
    sum_rows, square_rows = lax.psum(
        (
            jnp.sum(conv_sum, axis=1, keepdims=True),
            jnp.sum(conv_sum * conv_sum, axis=1, keepdims=True),
        ),
        "tp",
    )
    row_mean = sum_rows / channel_count
    centered = conv_sum - row_mean
    row_var = square_rows / channel_count - row_mean * row_mean
    conv_out = jax.nn.silu(centered * lax.rsqrt(row_var + 1e-05) * ln_gain + ln_bias).astype(
        jnp.bfloat16
    )
    return lax.psum_scatter(
        (
            jnp.dot(head_out, out_rec, preferred_element_type=jnp.float32)
            + jnp.dot(conv_out, out_conv, preferred_element_type=jnp.float32)
        ).astype(jnp.bfloat16),
        "tp",
        scatter_dimension=0,
        tiled=True,
    )


def solution(mesh):
    placed = (
        P(("sp", "tp"), None),
        P(),
        P("sp", "tp"),
        P("sp", "tp"),
        P("sp", "tp"),
        P("sp", "tp"),
        P("tp"),
        P("sp", "tp"),
        P(),
        P("sp", "tp"),
        P("sp", "tp"),
        P(None, "tp"),
        P("tp"),
        P("tp"),
        P("tp", "sp"),
        P("tp", "sp"),
    )
    return jax.shard_map(
        on_device, mesh=mesh, in_specs=placed, out_specs=P(("sp", "tp"), None), check_vma=False
    )
```

profile of v0, /device:TPU:0, one launch (start us, length us, event | category | flops | bytes accessed | tf_op | source)
XLA Modules:
  0.0 657.1 jit_solution(7365507671859252702)
XLA Ops:
  10.0 10.7 %all-gather.14.cloned.1.call-done = bf16[256,2048]{1,0:T(8,128)(2,1)} async-done(((bf16[128,2048]{1,0:T(8,128)(2,1)}), bf16[256,2048]{1,0:T(8,128)(2,1)}) %all-gather.14.cloned.1.call-update) | async-done | bytes 1048592 | tf_op jit(solution)/shard_map/all_gather | solution.py:148
  20.7 1.5 fusion.12
  22.2 62.8 %all-gather.20.cloned.1.call-done = bf16[2048,512]{1,0:T(8,128)(2,1)} async-done(((bf16[128,512]{1,0:T(8,128)(2,1)}), bf16[2048,512]{1,0:T(8,128)(2,1)}) %all-gather.20.cloned.1.call-update) | async-done | bytes 2097168 | tf_op jit(solution)/shard_map/all_gather | solution.py:137
  85.0 2.9 log-plus-one_add_fusion
  88.5 58.5 %all-gather.18.cloned.1.call-done = bf16[2048,512]{1,0:T(8,128)(2,1)} async-done(((bf16[128,512]{1,0:T(8,128)(2,1)}), bf16[2048,512]{1,0:T(8,128)(2,1)}) %all-gather.18.cloned.1.call-update) | async-done | bytes 2097168 | tf_op jit(solution)/shard_map/all_gather | solution.py:136
  147.0 2.8 divide_multiply_fusion.1
  150.0 58.9 %all-gather.16.cloned.1.call-done = bf16[2048,512]{1,0:T(8,128)(2,1)} async-done(((bf16[128,512]{1,0:T(8,128)(2,1)}), bf16[2048,512]{1,0:T(8,128)(2,1)}) %all-gather.16.cloned.1.call-update) | async-done | bytes 2097168 | tf_op jit(solution)/shard_map/all_gather | solution.py:138
  208.8 2.7 convolution_convert_fusion.5
  211.6 1.2 exponential_multiply_fusion.1
  212.8 1.0 fusion.33
  213.8 7.8 %while.45 = (s32[]{:T(128)}, f32[4,128,128]{2,1,0:T(8,128)S(1)}, f32[4,128]{1,0:T(4,128)S(1)}, f32[4,64,4,128]{3,1,2,0:T(8,128)}, f32[4,64,4,128]{3,1,0,2:T(8,12...) while((s32[]{:T(128)}, f32[4,128,128]{2,1,0:T(8,128)S(1)}, ...), condition=%wide.region_3.4_spmd.clone, body=%wide.region_2.3_spmd.clone.sunk | while | flops 50693120 | bytes 2374789 | solution.py:97
  214.6 1.0 fusion.73
  216.5 1.0 fusion.73
  218.5 1.0 fusion.73
  220.5 1.0 fusion.73
  225.3 38.8 %all-gather.2 = bf16[16,4,128]{2,1,0:T(4,128)(2,1)S(1)} all-gather(bf16[1,4,128]{2,1,0:T(4,128)(2,1)S(1)} %convert_bitcast_fusion), channel_id=2, replica_groups=mesh['sp'=16,'tp'=2] {'sp'}, dimensions={0}, use_global_device_ids=true | all-gather | bytes 17408 | tf_op jit(solution)/shard_map/all_gather | solution.py:16
  264.1 2.0 convolution_multiply_fusion
  266.8 3.9 all-gather.22.cloned.1.call-done
  270.7 2.8 divide_multiply_fusion
  273.7 58.9 %all-gather.32.cloned.1.call-done = bf16[64,128,128]{2,1,0:T(8,128)(2,1)} async-done(((bf16[4,128,128]{2,1,0:T(8,128)(2,1)}), bf16[64,128,128]{2,1,0:T(8,128)(2,1)}) %all-gather.32.cloned.1.call-update) | async-done | bytes 2097168 | tf_op jit(solution)/shard_map/all_gather | solution.py:16
  332.6 18.4 %while.46 = (s32[]{:T(128)}, f32[4,128,128]{2,1,0:T(8,128)S(1)}, s32[]{:T(128)}, bf16[16,4,128]{2,1,0:T(4,128)(2,1)S(1)}, bf16[16,4,128,128]{3,2,1,0:T(8,128)(2,1)}, /*index=5*/s32[]{:T(128)}, s32[]{:T(128)}) while((s32[]{:T(128)}, f32[4,128,128]{2,1,0:T(8,128)S(1)}, s32[]{:T(128)}, bf16[16,4,128]{2,1,0:T(4,128)(2,1)S(1)}, ...), condition=%wide.region_5.6_spmd.clone, body=%wide.region_4.5_spmd.clone.sunk | while | flops 328196 | bytes 660585 | solution.py:33
  332.6 1.1 fusion.74
  333.7 1.1 fusion.74
  334.9 1.1 fusion.74
  336.0 1.1 fusion.74
  337.2 1.1 fusion.74
  338.3 1.1 fusion.74
  339.5 1.1 fusion.74
  340.6 1.1 fusion.74
  341.8 1.1 fusion.74
  342.9 1.1 fusion.74
  344.1 1.1 fusion.74
  345.2 1.1 fusion.74
  346.4 1.1 fusion.74
  347.5 1.1 fusion.74
  348.7 1.1 fusion.74
  349.8 1.1 fusion.74
  350.9 1.7 multiply_reduce_fusion.1
  352.7 57.1 %all-gather.26.cloned.1.call-done = bf16[2048,1024]{1,0:T(8,128)(2,1)} async-done(((bf16[128,1024]{1,0:T(8,128)(2,1)}), bf16[2048,1024]{1,0:T(8,128)(2,1)}) %all-gather.26.cloned.1.call-update) | async-done | bytes 4194320 | tf_op jit(solution)/shard_map/all_gather | solution.py:140
  409.8 4.8 fusion.22
  414.6 72.2 %all-gather.28.cloned.1.call-done = bf16[2048,1024]{1,0:T(8,128)(2,1)} async-done(((bf16[128,1024]{1,0:T(8,128)(2,1)}), bf16[2048,1024]{1,0:T(8,128)(2,1)}) %all-gather.28.cloned.1.call-update) | async-done | bytes 4194320 | tf_op jit(solution)/shard_map/all_gather | solution.py:141
  486.8 4.2 fusion.21
  491.0 3.5 collective-permute-start
  494.6 1.6 collective-permute-done
  496.4 40.1 %while.47 = (s32[]{:T(128)}, f32[256,1024]{1,0:T(8,128)S(1)}, f32[31,1024]{1,0:T(8,128)}, f32[286,1024]{1,0:T(8,128)S(1)}, s32[]{:T(128)}, /*index=5*/s32[]{:T(128)}) while((s32[]{:T(128)}, f32[256,1024]{1,0:T(8,128)S(1)}, f32[31,1024]{1,0:T(8,128)}, f32[286,1024]{1,0:T(8,128)S(1)}, s32[]{:T(128)}, /*index=5*/s32[]{:T(128)}) %tuple.92), condition=%wide.region_8.9_spmd.clone, body=%wide.region_7.8_spmd.clone.sunk | while | flops 786435 | bytes 3158103 | solution.py:199
  496.4 0.8 constant_dynamic-slice_fusion.6
  497.7 0.8 constant_dynamic-slice_fusion.6
  499.0 0.8 constant_dynamic-slice_fusion.6
  500.3 0.8 constant_dynamic-slice_fusion.6
  501.6 0.8 constant_dynamic-slice_fusion.6
  502.9 0.8 constant_dynamic-slice_fusion.6
  504.2 0.8 constant_dynamic-slice_fusion.6
  506.8 0.8 constant_dynamic-slice_fusion.6
  510.6 0.8 constant_dynamic-slice_fusion.6
  519.7 0.8 constant_dynamic-slice_fusion.6
  521.0 0.8 constant_dynamic-slice_fusion.6
  526.2 0.8 constant_dynamic-slice_fusion.6
  528.7 0.8 constant_dynamic-slice_fusion.6
  536.7 2.5 all-reduce
  539.2 37.6 %all-gather.30.cloned.1.call-done = bf16[1024,2048]{1,0:T(8,128)(2,1)} async-done(((bf16[1024,128]{1,0:T(8,128)(2,1)}), bf16[1024,2048]{1,0:T(8,128)(2,1)}) %all-gather.30.cloned.1.call-update) | async-done | bytes 4194320 | tf_op jit(solution)/shard_map/all_gather | solution.py:143
  576.8 3.7 fusion.32
  580.5 60.0 %all-gather.24.cloned.1.call-done = bf16[512,2048]{1,0:T(8,128)(2,1)} async-done(((bf16[512,128]{1,0:T(8,128)(2,1)}), bf16[512,2048]{1,0:T(8,128)(2,1)}) %all-gather.24.cloned.1.call-update) | async-done | bytes 2097168 | tf_op jit(solution)/shard_map/all_gather | solution.py:142
  640.5 3.3 fusion.11
  643.9 6.7 %reduce-scatter.2.cloned.1.call-done = bf16[128,2048]{1,0:T(8,128)(2,1)} async-done(((bf16[256,2048]{1,0:T(8,128)(2,1)}), bf16[128,2048]{1,0:T(8,128)(2,1)}) %reduce-scatter.2.cloned.1.call-update) | async-done | bytes 524304 | tf_op jit(solution)/shard_map/reduce_scatter | solution.py:214
  (143 shorter events, 42.2 us)
Async XLA Ops:
  6.5 78.5 %copy-start.3 = (f32[2048]{0:T(1024)S(1)}, f32[2048]{0:T(1024)}, u32[]{:S(2)}) copy-start(f32[2048]{0:T(1024)} %param.23) | copy-start | bytes 24580
  6.5 78.5 %copy-start.6 = (f32[512]{0:T(512)S(1)}, f32[512]{0:T(512)}, u32[]{:S(2)}) copy-start(f32[512]{0:T(512)} %param.28) | copy-start | bytes 6148
  6.5 78.5 %copy-start.2 = (f32[256,512]{1,0:T(8,128)S(1)}, f32[256,512]{1,0:T(8,128)}, u32[]{:S(2)}) copy-start(f32[256,512]{1,0:T(8,128)} %param.29) | copy-start | bytes 1572868
  6.5 14.1 %all-gather.14.cloned.1.call-start = ((), (), s32[]{:S(2)}) async-start(), calls=%async_computation.1 | async-start | bytes 1572864 | tf_op jit(solution)/shard_map/all_gather | solution.py:148
  7.3 77.8 %all-gather.20.cloned.1.call-start = ((), (), s32[]{:S(2)}) async-start(), calls=%async_computation.4 | async-start | bytes 2228224 | tf_op jit(solution)/shard_map/all_gather | solution.py:137
  8.0 139.0 %all-gather.18.cloned.1.call-start = ((), (), s32[]{:S(2)}) async-start(), calls=%async_computation.3 | async-start | bytes 2228224 | tf_op jit(solution)/shard_map/all_gather | solution.py:136
  8.7 200.1 %all-gather.16.cloned.1.call-start = ((), (), s32[]{:S(2)}) async-start(), calls=%async_computation.2 | async-start | bytes 2228224 | tf_op jit(solution)/shard_map/all_gather | solution.py:138
  9.3 261.4 %all-gather.22.cloned.1.call-start = ((), (), s32[]{:S(2)}) async-start(), calls=%async_computation.5 | async-start | bytes 2228224 | tf_op jit(solution)/shard_map/all_gather | solution.py:139
  9.9 322.7 %all-gather.32.cloned.1.call-start = ((), (), s32[]{:S(2)}) async-start(), calls=%async_computation.11 | async-start | bytes 2228224 | tf_op jit(solution)/shard_map/all_gather | solution.py:16
  221.7 44.5 %copy-start = (f32[4,64,4,128]{3,1,2,0:T(8,128)S(1)}, f32[4,64,4,128]{3,1,2,0:T(8,128)}, u32[]{:S(2)}) copy-start(f32[4,64,4,128]{3,1,2,0:T(8,128)} %get-tuple-element.228) | copy-start | bytes 1572868
  222.4 187.4 %all-gather.26.cloned.1.call-start = ((), (), s32[]{:S(2)}) async-start(), calls=%async_computation.7 | async-start | bytes 4456448 | tf_op jit(solution)/shard_map/all_gather | solution.py:140
  223.1 263.6 %all-gather.28.cloned.1.call-start = ((), (), s32[]{:S(2)}) async-start(), calls=%async_computation.8 | async-start | bytes 4456448 | tf_op jit(solution)/shard_map/all_gather | solution.py:141
  223.9 352.9 %all-gather.30.cloned.1.call-start = ((), (), s32[]{:S(2)}) async-start(), calls=%async_computation.9 | async-start | bytes 4456448 | tf_op jit(solution)/shard_map/all_gather | solution.py:143
  224.6 415.9 %all-gather.24.cloned.1.call-start = ((), (), s32[]{:S(2)}) async-start(), calls=%async_computation.6 | async-start | bytes 2228224 | tf_op jit(solution)/shard_map/all_gather | solution.py:142
  225.2 425.4 %reduce-scatter.2.cloned.1.call-start = ((), (), s32[]{:S(2)}) async-start(), calls=%async_computation.10 | async-start | bytes 1572864 | tf_op jit(solution)/shard_map/reduce_scatter | solution.py:214
  414.6 79.9 %copy-start.1 = (f32[128]{0:T(128)S(1)}, f32[128]{0:T(128)}, u32[]{:S(2)}) copy-start(f32[128]{0:T(128)} %param.30) | copy-start | bytes 1540
  491.0 5.2 collective-permute-start
  496.4 80.4 %copy-start.4 = (f32[1024]{0:T(1024)S(1)}, f32[1024]{0:T(1024)}, u32[]{:S(2)}) copy-start(f32[1024]{0:T(1024)} %param.35) | copy-start | bytes 12292
  496.4 80.4 %copy-start.5 = (f32[1024]{0:T(1024)S(1)}, f32[1024]{0:T(1024)}, u32[]{:S(2)}) copy-start(f32[1024]{0:T(1024)} %param.34) | copy-start | bytes 12292
Sparse Core Ops, SparseCore 0:
  8.9 11.7 all-gather.13
  23.4 61.5 all-gather.19
  87.8 59.1 all-gather.17
  149.6 59.1 all-gather.15
  211.5 59.2 all-gather.21
  273.4 59.1 all-gather.31
  335.3 74.3 all-gather.25
  412.5 74.1 all-gather.27
  489.5 87.3 all-gather.29
  579.4 61.1 all-gather.23
  644.0 6.5 reduce-scatter.1
where the time goes:
time: 660 us; the launch traced here: 657 us
  waiting for transfers between devices  495 us (75%)
  blocking collectives  41.3 us (6%)
  other arithmetic  41 us (6%)
  matrix products  36.4 us (6%)
  local copies, waits for them, and re-layouts  25 us (4%)
  between operations  13.6 us (2%)
    all_gather x1, waiting for transfers between devices, on_device(): lax.all_gather(w_glu_gate, 'sp', axis=0, tiled=True)  72.2 us
    all_gather x1, waiting for transfers between devices, on_device(): lax.all_gather(w_forget, 'sp', axis=0, tiled=True)  62.8 us
    all_gather x1, waiting for transfers between devices, on_device(): lax.all_gather(w_out_rec, 'sp', axis=1, tiled=True)  60 us
    all_gather x1, waiting for transfers between devices, on_device(): lax.all_gather(w_value, 'sp', axis=0, tiled=True)  58.9 us
    all_gather x1, waiting for transfers between devices, prefix(): lax.all_gather(part.astype(kind), axis)  58.9 us
    all_gather x1, waiting for transfers between devices, on_device(): lax.all_gather(w_query, 'sp', axis=0, tiled=True)  58.5 us
    all_gather x1, waiting for transfers between devices, on_device(): lax.all_gather(w_glu_value, 'sp', axis=0, tiled=True)  57.1 us
    all_gather x1, blocking collectives, prefix(): lax.all_gather(part.astype(kind), axis)  38.8 us
  transfers between devices with their start and end apart: 12, of which 12 were waited for; matrix products, arithmetic and copies ran while one was open for 15% of the time, Pallas kernels for 0%

commit v1 on v0

--- a/solution.py
+++ b/solution.py
@@ -1,3 +1,4 @@
+import functools
 import jax
 import jax.numpy as jnp
 from jax import lax
@@ -8,6 +9,17 @@
 KERNEL = 31
 BLOCK = 64
 exact_precision = lax.Precision.HIGHEST
+
+
+def deliver_object(z, k_dim):
+    by_rank = []
+    for _ in range(lax.axis_size("sp")):
+        by_rank.append(z)
+    now = jnp.concatenate(lax.all_to_all(jnp.stack(by_rank, axis=0), "sp", 0, 0), axis=k_dim)
+    return now
+
+
+form_the_views = functools.partial(deliver_object, k_dim=1)
 
 
 def prefix(value, axis, combine, identity):
@@ -139,7 +151,7 @@
         lax.all_gather(w_outgate, "sp", axis=0, tiled=True),
         lax.all_gather(w_glu_value, "sp", axis=0, tiled=True),
         lax.all_gather(w_glu_gate, "sp", axis=0, tiled=True),
-        lax.all_gather(w_out_rec, "sp", axis=1, tiled=True),
+        form_the_views(w_out_rec),
         lax.all_gather(w_out_conv, "sp", axis=1, tiled=True),
     )
     full_in = gathered[:6]

time: 660 us -> 621 us (0.941)
  waiting for transfers between devices: 495 us -> 408 us
  blocking collectives: 41.3 us -> 83.9 us
    all_gather x1 -> x0, waiting for transfers between devices: 60 us -> none  [on_device(): lax.all_gather(w_out_rec, 'sp', axis=1, tiled=True)]
    all_gather x1, blocking collectives: 38.8 us -> 81.5 us  [prefix(): lax.all_gather(part.astype(kind), axis)]
    all_gather x1, waiting for transfers between devices: 58.9 us -> 36.4 us  [prefix(): lax.all_gather(part.astype(kind), axis)]
  transfers between devices with their start and end apart: 12 -> 12, of which waited for: 12 -> 10; matrix products, arithmetic and copies ran while one was open for 15% -> 16% of each run, Pallas kernels for 0% -> 0%
where the time goes in v1:
time: 621 us; the launch traced here: 618 us
  waiting for transfers between devices  408 us (66%)
  blocking collectives  83.9 us (14%)
  other arithmetic  41 us (7%)
  matrix products  34.7 us (6%)
  local copies, waits for them, and re-layouts  26.7 us (4%)
  between operations  13.9 us (2%)
  starting transfers between devices  8.48 us (1%)
    all_gather x1, blocking collectives, prefix(): lax.all_gather(part.astype(kind), axis)  81.5 us
    all_gather x1, waiting for transfers between devices, on_device(): lax.all_gather(w_glu_gate, 'sp', axis=0, tiled=True)  72.2 us
    all_gather x1, waiting for transfers between devices, on_device(): lax.all_gather(w_forget, 'sp', axis=0, tiled=True)  62.8 us
    all_gather x1, waiting for transfers between devices, on_device(): lax.all_gather(w_value, 'sp', axis=0, tiled=True)  59.2 us
    all_gather x1, waiting for transfers between devices, on_device(): lax.all_gather(w_query, 'sp', axis=0, tiled=True)  58.5 us
    all_gather x1, waiting for transfers between devices, on_device(): lax.all_gather(w_glu_value, 'sp', axis=0, tiled=True)  57.1 us
    all_gather x1, waiting for transfers between devices, on_device(): lax.all_gather(w_out_conv, 'sp', axis=1, tiled=True)  37.9 us
    all_gather x1, waiting for transfers between devices, prefix(): lax.all_gather(part.astype(kind), axis)  36.4 us
  transfers between devices with their start and end apart: 12, of which 10 were waited for; matrix products, arithmetic and copies ran while one was open for 16% of the time, Pallas kernels for 0%

profile of v1, /device:TPU:0, one launch (start us, length us, event | category | flops | bytes accessed | tf_op | source)
XLA Modules:
  0.0 618.5 jit_solution(4115681683504254443)
XLA Ops:
  10.0 10.7 %all-gather.13.cloned.1.call-done = bf16[256,2048]{1,0:T(8,128)(2,1)} async-done(((bf16[128,2048]{1,0:T(8,128)(2,1)}), bf16[256,2048]{1,0:T(8,128)(2,1)}) %all-gather.13.cloned.1.call-update) | async-done | bytes 1048592 | tf_op jit(solution)/shard_map/all_gather | solution.py:160
  20.7 1.5 fusion.12
  22.2 62.8 %all-gather.19.cloned.1.call-done = bf16[2048,512]{1,0:T(8,128)(2,1)} async-done(((bf16[128,512]{1,0:T(8,128)(2,1)}), bf16[2048,512]{1,0:T(8,128)(2,1)}) %all-gather.19.cloned.1.call-update) | async-done | bytes 2097168 | tf_op jit(solution)/shard_map/all_gather | solution.py:149
  85.0 2.9 log-plus-one_add_fusion
  88.5 58.5 %all-gather.17.cloned.1.call-done = bf16[2048,512]{1,0:T(8,128)(2,1)} async-done(((bf16[128,512]{1,0:T(8,128)(2,1)}), bf16[2048,512]{1,0:T(8,128)(2,1)}) %all-gather.17.cloned.1.call-update) | async-done | bytes 2097168 | tf_op jit(solution)/shard_map/all_gather | solution.py:148
  147.0 2.4 divide_multiply_fusion.1
  149.6 59.2 %all-gather.15.cloned.1.call-done = bf16[2048,512]{1,0:T(8,128)(2,1)} async-done(((bf16[128,512]{1,0:T(8,128)(2,1)}), bf16[2048,512]{1,0:T(8,128)(2,1)}) %all-gather.15.cloned.1.call-update) | async-done | bytes 2097168 | tf_op jit(solution)/shard_map/all_gather | solution.py:150
  208.8 2.7 convolution_convert_fusion.5
  211.6 1.2 exponential_multiply_fusion.1
  212.8 1.0 fusion.33
  213.8 7.8 %while.45 = (s32[]{:T(128)}, f32[4,128,128]{2,1,0:T(8,128)S(1)}, f32[4,128]{1,0:T(4,128)S(1)}, f32[4,64,4,128]{3,1,2,0:T(8,128)}, f32[4,64,4,128]{3,1,0,2:T(8,12...) while((s32[]{:T(128)}, f32[4,128,128]{2,1,0:T(8,128)S(1)}, ...), condition=%wide.region_3.4_spmd.clone, body=%wide.region_2.3_spmd.clone.sunk | while | flops 50693120 | bytes 2374789 | solution.py:109
  214.6 1.0 fusion.73
  216.5 1.0 fusion.73
  218.5 1.0 fusion.73
  220.4 1.0 fusion.73
  224.0 1.5 stack.2
  225.5 4.6 all-to-all-start
  231.0 81.5 %all-gather.2 = bf16[16,4,128]{2,1,0:T(4,128)(2,1)S(1)} all-gather(bf16[1,4,128]{2,1,0:T(4,128)(2,1)S(1)} %convert_bitcast_fusion), channel_id=2, replica_groups=mesh['sp'=16,'tp'=2] {'sp'}, dimensions={0}, use_global_device_ids=true | all-gather | bytes 17408 | tf_op jit(solution)/shard_map/all_gather | solution.py:28
  312.4 1.0 convolution_multiply_fusion
  314.1 2.8 divide_multiply_fusion
  317.1 36.4 %all-gather.29.cloned.1.call-done = bf16[64,128,128]{2,1,0:T(8,128)(2,1)} async-done(((bf16[4,128,128]{2,1,0:T(8,128)(2,1)}), bf16[64,128,128]{2,1,0:T(8,128)(2,1)}) %all-gather.29.cloned.1.call-update) | async-done | bytes 2097168 | tf_op jit(solution)/shard_map/all_gather | solution.py:28
  353.5 18.4 %while.46 = (s32[]{:T(128)}, f32[4,128,128]{2,1,0:T(8,128)S(1)}, s32[]{:T(128)}, bf16[16,4,128]{2,1,0:T(4,128)(2,1)S(1)}, bf16[16,4,128,128]{3,2,1,0:T(8,128)(2,1)}, /*index=5*/s32[]{:T(128)}, s32[]{:T(128)}) while((s32[]{:T(128)}, f32[4,128,128]{2,1,0:T(8,128)S(1)}, s32[]{:T(128)}, bf16[16,4,128]{2,1,0:T(4,128)(2,1)S(1)}, ...), condition=%wide.region_5.6_spmd.clone, body=%wide.region_4.5_spmd.clone.sunk | while | flops 328196 | bytes 660585 | solution.py:45
  353.5 1.1 fusion.74
  354.7 1.1 fusion.74
  355.8 1.1 fusion.74
  357.0 1.1 fusion.74
  358.1 1.1 fusion.74
  359.3 1.1 fusion.74
  360.4 1.1 fusion.74
  361.6 1.1 fusion.74
  362.7 1.1 fusion.74
  363.9 1.1 fusion.74
  365.0 1.1 fusion.74
  366.2 1.1 fusion.74
  367.3 1.1 fusion.74
  368.5 1.1 fusion.74
  369.6 1.1 fusion.74
  370.8 1.1 fusion.74
  371.9 1.7 multiply_reduce_fusion.1
  373.6 57.1 %all-gather.23.cloned.1.call-done = bf16[2048,1024]{1,0:T(8,128)(2,1)} async-done(((bf16[128,1024]{1,0:T(8,128)(2,1)}), bf16[2048,1024]{1,0:T(8,128)(2,1)}) %all-gather.23.cloned.1.call-update) | async-done | bytes 4194320 | tf_op jit(solution)/shard_map/all_gather | solution.py:152
  430.7 4.8 fusion.22
  435.5 72.2 %all-gather.25.cloned.1.call-done = bf16[2048,1024]{1,0:T(8,128)(2,1)} async-done(((bf16[128,1024]{1,0:T(8,128)(2,1)}), bf16[2048,1024]{1,0:T(8,128)(2,1)}) %all-gather.25.cloned.1.call-update) | async-done | bytes 4194320 | tf_op jit(solution)/shard_map/all_gather | solution.py:153
  507.7 3.9 fusion.21
  511.6 3.5 collective-permute-start
  515.3 1.6 collective-permute-done
  517.0 40.1 %while.47 = (s32[]{:T(128)}, f32[256,1024]{1,0:T(8,128)S(1)}, f32[31,1024]{1,0:T(8,128)}, f32[286,1024]{1,0:T(8,128)S(1)}, s32[]{:T(128)}, /*index=5*/s32[]{:T(128)}) while((s32[]{:T(128)}, f32[256,1024]{1,0:T(8,128)S(1)}, f32[31,1024]{1,0:T(8,128)}, f32[286,1024]{1,0:T(8,128)S(1)}, s32[]{:T(128)}, /*index=5*/s32[]{:T(128)}) %tuple.92), condition=%wide.region_8.9_spmd.clone, body=%wide.region_7.8_spmd.clone.sunk | while | flops 786435 | bytes 3158103 | solution.py:211
  517.0 0.8 constant_dynamic-slice_fusion.6
  518.3 0.8 constant_dynamic-slice_fusion.6
  519.6 0.8 constant_dynamic-slice_fusion.6
  520.9 0.8 constant_dynamic-slice_fusion.6
  522.2 0.8 constant_dynamic-slice_fusion.6
  523.5 0.8 constant_dynamic-slice_fusion.6
  524.8 0.8 constant_dynamic-slice_fusion.6
  526.1 0.8 constant_dynamic-slice_fusion.6
  531.3 0.8 constant_dynamic-slice_fusion.6
  540.3 0.8 constant_dynamic-slice_fusion.6
  541.6 0.8 constant_dynamic-slice_fusion.6
  546.8 0.8 constant_dynamic-slice_fusion.6
  549.4 0.8 constant_dynamic-slice_fusion.6
  557.4 2.5 all-reduce
  559.8 37.9 %all-gather.27.cloned.1.call-done = bf16[1024,2048]{1,0:T(8,128)(2,1)} async-done(((bf16[1024,128]{1,0:T(8,128)(2,1)}), bf16[1024,2048]{1,0:T(8,128)(2,1)}) %all-gather.27.cloned.1.call-update) | async-done | bytes 4194320 | tf_op jit(solution)/shard_map/all_gather | solution.py:155
  597.8 3.7 fusion.32
  601.5 3.3 fusion.11
  604.9 6.7 %reduce-scatter.2.cloned.1.call-done = bf16[128,2048]{1,0:T(8,128)(2,1)} async-done(((bf16[256,2048]{1,0:T(8,128)(2,1)}), bf16[128,2048]{1,0:T(8,128)(2,1)}) %reduce-scatter.2.cloned.1.call-update) | async-done | bytes 524304 | tf_op jit(solution)/shard_map/reduce_scatter | solution.py:226
  (154 shorter events, 41.8 us)
Async XLA Ops:
  6.5 78.5 %copy-start.7 = (f32[2048]{0:T(1024)S(1)}, f32[2048]{0:T(1024)}, u32[]{:S(2)}) copy-start(f32[2048]{0:T(1024)} %param.23) | copy-start | bytes 24580
  6.5 78.5 %copy-start.11 = (f32[512]{0:T(512)S(1)}, f32[512]{0:T(512)}, u32[]{:S(2)}) copy-start(f32[512]{0:T(512)} %param.28) | copy-start | bytes 6148
  6.5 78.5 %copy-start.6 = (f32[256,512]{1,0:T(8,128)S(1)}, f32[256,512]{1,0:T(8,128)}, u32[]{:S(2)}) copy-start(f32[256,512]{1,0:T(8,128)} %param.29) | copy-start | bytes 1572868
  6.5 14.1 %all-gather.13.cloned.1.call-start = ((), (), s32[]{:S(2)}) async-start(), calls=%async_computation.2 | async-start | bytes 1572864 | tf_op jit(solution)/shard_map/all_gather | solution.py:160
  7.3 77.8 %all-gather.19.cloned.1.call-start = ((), (), s32[]{:S(2)}) async-start(), calls=%async_computation.5 | async-start | bytes 2228224 | tf_op jit(solution)/shard_map/all_gather | solution.py:149
  8.0 139.0 %all-gather.17.cloned.1.call-start = ((), (), s32[]{:S(2)}) async-start(), calls=%async_computation.4 | async-start | bytes 2228224 | tf_op jit(solution)/shard_map/all_gather | solution.py:148
  8.7 200.1 %all-gather.15.cloned.1.call-start = ((), (), s32[]{:S(2)}) async-start(), calls=%async_computation.3 | async-start | bytes 2228224 | tf_op jit(solution)/shard_map/all_gather | solution.py:150
  9.3 304.8 %all-gather.21.cloned.1.call-start = ((), (), s32[]{:S(2)}) async-start(), calls=%async_computation.6 | async-start | bytes 2228224 | tf_op jit(solution)/shard_map/all_gather | solution.py:151
  9.9 343.6 %all-gather.29.cloned.1.call-start = ((), (), s32[]{:S(2)}) async-start(), calls=%async_computation.11 | async-start | bytes 2228224 | tf_op jit(solution)/shard_map/all_gather | solution.py:28
  88.0 59.0 %copy-start.1 = (bf16[256,2048]{1,0:T(8,128)(2,1)S(1)}, bf16[256,2048]{1,0:T(8,128)(2,1)}, u32[]{:S(2)}) copy-start(bf16[256,2048]{1,0:T(8,128)(2,1)} %all-gather.13.cloned.1.call-done) | copy-start | bytes 3145732
  213.8 10.0 %copy-start.4 = (bf16[512,128]{1,0:T(8,128)(2,1)S(1)}, bf16[512,128]{1,0:T(8,128)(2,1)}, u32[]{:S(2)}) copy-start(bf16[512,128]{1,0:T(8,128)(2,1)} %param.36) | copy-start | bytes 393220
  222.3 208.4 %all-gather.23.cloned.1.call-start = ((), (), s32[]{:S(2)}) async-start(), calls=%async_computation.7 | async-start | bytes 4456448 | tf_op jit(solution)/shard_map/all_gather | solution.py:152
  223.1 284.6 %all-gather.25.cloned.1.call-start = ((), (), s32[]{:S(2)}) async-start(), calls=%async_computation.8 | async-start | bytes 4456448 | tf_op jit(solution)/shard_map/all_gather | solution.py:153
  225.5 86.9 %copy-start = (f32[4,64,4,128]{3,2,1,0:T(4,128)S(1)}, f32[4,64,4,128]{3,2,1,0:T(4,128)}, u32[]{:S(2)}) copy-start(f32[4,64,4,128]{3,2,1,0:T(4,128)} %get-tuple-element.371) | copy-start | bytes 1572868
  225.5 87.9 %copy-start.3 = (f32[4,64,4,128]{3,1,2,0:T(8,128)S(1)}, f32[4,64,4,128]{3,1,2,0:T(8,128)}, u32[]{:S(2)}) copy-start(f32[4,64,4,128]{3,1,2,0:T(8,128)} %get-tuple-element.228) | copy-start | bytes 1572868
  225.5 376.0 %all-to-all-start = ((bf16[16,512,128]{1,2,0:T(8,128)(2,1)}), bf16[16,512,128]{1,2,0:T(8,128)(2,1)}, u32[]{:S(2)}, u32[]{:S(2)}) async-start(bf16[16,512,128]{1,2,0:T(8,128)(2,1)} %stack.2), calls=%async_computation | async-start | bytes 4194304 | tf_op jit(solution)/shard_map/all_to_all | solution.py:18
  230.1 367.6 %all-gather.27.cloned.1.call-start = ((), (), s32[]{:S(2)}) async-start(), calls=%async_computation.9 | async-start | bytes 4456448 | tf_op jit(solution)/shard_map/all_gather | solution.py:155
  230.9 380.7 %reduce-scatter.2.cloned.1.call-start = ((), (), s32[]{:S(2)}) async-start(), calls=%async_computation.10 | async-start | bytes 1572864 | tf_op jit(solution)/shard_map/reduce_scatter | solution.py:226
  313.4 0.7 copy-start.8
  373.6 134.1 %copy-start.2 = (bf16[256,2048]{1,0:T(8,128)(2,1)S(1)}, bf16[256,2048]{1,0:T(8,128)(2,1)}, u32[]{:S(2)}) copy-start(bf16[256,2048]{1,0:T(8,128)(2,1)} %all-gather.13.cloned.1.call-done) | copy-start | bytes 3145732
  435.5 79.6 %copy-start.5 = (f32[128]{0:T(128)S(1)}, f32[128]{0:T(128)}, u32[]{:S(2)}) copy-start(f32[128]{0:T(128)} %param.30) | copy-start | bytes 1540
  511.6 5.2 collective-permute-start
  517.0 80.8 %copy-start.9 = (f32[1024]{0:T(1024)S(1)}, f32[1024]{0:T(1024)}, u32[]{:S(2)}) copy-start(f32[1024]{0:T(1024)} %param.35) | copy-start | bytes 12292
  517.0 80.8 %copy-start.10 = (f32[1024]{0:T(1024)S(1)}, f32[1024]{0:T(1024)}, u32[]{:S(2)}) copy-start(f32[1024]{0:T(1024)} %param.34) | copy-start | bytes 12292
Sparse Core Ops, SparseCore 0:
  8.9 11.7 all-gather.12
  23.4 61.5 all-gather.18
  87.8 59.1 all-gather.16
  149.6 59.1 all-gather.14
  211.5 78.1 all-gather.20
  292.3 61.2 all-gather.28
  356.3 74.3 all-gather.22
  433.5 74.1 all-gather.24
  510.4 87.3 all-gather.26
  605.0 6.5 reduce-scatter.1
